TPU v7x, 32 devices: a whole 2x2x4 slice. The times are simulated.
32 devices in a mesh: sp: 4 (over z), fs: 4 (over y, x), tp: 2 (over core).
Axes of the slice: x: 2, y: 2, z: 4, core: 2. Of those that a mesh axis runs over, the one named last changes fastest.
Arguments:
- tokens: bfloat16 [4, 512, 2048], P('fs', ('sp', 'tp')), may hold values from -6 to 6
- norm_gain: float32 [2048], replicated, may hold values from 0.1 to 1.9
- rec_query: bfloat16 [2048, 512], P('sp', 'tp'), may hold values from -0.125 to 0.125
- rec_input: bfloat16 [2048, 512], P('sp', 'tp'), may hold values from -0.125 to 0.125
- rec_forward: bfloat16 [2048, 512], P('sp', 'tp'), may hold values from -0.125 to 0.125
- rec_backward: bfloat16 [2048, 512], P('sp', 'tp'), may hold values from -0.125 to 0.125
- forget_gap: float32 [2, 512], P(None, 'tp'), may hold values from 0 to 0.06
- log_decay: float32 [4, 2, 4, 512], P('fs', None, 'tp', 'sp'), may hold values from -0.7 to 0
- rec_gain: float32 [512], P('tp'), may hold values from 0.1 to 1.9
- conv_value: bfloat16 [2048, 512], P('sp', 'tp'), may hold values from -0.125 to 0.125
- conv_gate: bfloat16 [2048, 512], P('sp', 'tp'), may hold values from -0.125 to 0.125
- conv_kernel: bfloat16 [31, 512], P(None, 'tp'), may hold values from -3.1 to 3.1
- conv_gain: float32 [512], P('tp'), may hold values from 0.1 to 1.9
- out_rec: bfloat16 [512, 2048], P('tp', 'sp'), may hold values from -0.1875 to 0.1875
- out_conv: bfloat16 [512, 2048], P('tp', 'sp'), may hold values from -0.1875 to 0.1875
Outputs:
- mixed: bfloat16 [4, 512, 2048], P('fs', ('sp', 'tp'))
All inputs are finite; a program needn't handle non-finite values.
Results may differ from a plain program's by a relative error of at most 0.017.
Values may be sent and summed in bfloat16 or wider, within the bound.
A program may use at most 64 MiB of HBM per device.

v0:
```python
import functools

import jax
import jax.numpy as jnp
from jax import lax
from jax.experimental import pallas as pl
from jax.experimental.pallas import tpu as pltpu
from jax.sharding import PartitionSpec as P

KD = 128
VD = 128
BLOCK = 64


EPS = 1e-06
HIGH = lax.Precision.HIGHEST


def entering(x, axis, join, neutral, backward):
    count = lax.axis_size(axis)
    place = lax.axis_index(axis)
    ahead = count - 1 - place if backward else place
    gathered = jax.tree.map(
        lambda a, kind: lax.all_gather(a.astype(kind), axis), x, (jnp.bfloat16, jnp.bfloat16)
    )
    state = jax.tree.map(lambda a, e: jnp.zeros_like(a) + jnp.asarray(e, a.dtype), x, neutral)

    def one(lap, state):
        source = count - 1 - lap if backward else lap
        return join(
            state,
            jax.tree.map(
                lambda a, own: lax.dynamic_index_in_dim(a, source, 0, False).astype(own.dtype),
                gathered,
                x,
            ),
        )

    return lax.fori_loop(0, ahead, one, state)


def padded_2(cells, sides, width):
    for axis, dim in sides:
        count = lax.axis_size(axis)
        ends = count - 1
        head = lax.slice_in_dim(cells, 0, width, axis=dim)
        tail = lax.slice_in_dim(cells, cells.shape[dim] - width, cells.shape[dim], axis=dim)
        cells = jnp.concatenate(
            [
                lax.ppermute(tail, axis, [(i, (i + 1) % count) for i in range(ends)]),
                cells,
                lax.ppermute(head, axis, [((i + 1) % count, i) for i in range(ends)]),
            ],
            axis=dim,
        )
    return cells


def block_pass(queries, key_rows, value_rows, log_gate):
    heads_n, length_n, key_dim = queries.shape
    value_dim = value_rows.shape[-1]
    blocks = length_n // BLOCK

    def split_blocks(tensor):
        return tensor.reshape(heads_n, blocks, BLOCK, tensor.shape[-1]).transpose(1, 0, 2, 3)

    def join_blocks(tensor):
        return tensor.transpose(1, 0, 2, 3).reshape(heads_n, length_n, tensor.shape[-1])

    lower_mask = jnp.tril(jnp.ones((BLOCK, BLOCK), bool))

    def advance(carried, inputs):
        states, offset = carried
        query_b, key_b, value_b, gate_b = inputs
        cumulative = jnp.cumsum(gate_b, axis=1)
        query_g = query_b * jnp.exp(cumulative)
        key_g = key_b * jnp.exp(-cumulative)
        scores = jnp.einsum("htd,hsd->hts", query_g, key_g, precision=HIGH)
        scores = jnp.where(lower_mask, scores, 0.0)
        result = jnp.einsum("hts,hse->hte", scores, value_b, precision=HIGH)
        result = result + jnp.einsum("htd,hde->hte", query_g, states, precision=HIGH)
        last_g = cumulative[:, -1, :]
        weighted = key_b * jnp.exp(last_g[:, None, :] - cumulative)
        states = jnp.exp(last_g)[:, :, None] * states + jnp.einsum(
            "hsd,hse->hde", weighted, value_b, precision=HIGH
        )
        decayed = query_b * jnp.exp(offset[:, None, :] + cumulative)
        return ((states, offset + last_g), (result, decayed))

    start_state = jnp.zeros((heads_n, key_dim, value_dim), jnp.float32)
    start_offset = jnp.zeros((heads_n, key_dim), jnp.float32)
    inputs = (
        split_blocks(queries),
        split_blocks(key_rows),
        split_blocks(value_rows),
        split_blocks(log_gate),
    )
    final_pair, outputs = lax.scan(advance, (start_state, start_offset), inputs)
    return (join_blocks(outputs[0]), join_blocks(outputs[1]), final_pair[1], final_pair[0])


def chain_combine(first_part, second_part):
    return (
        first_part[0] * second_part[0],
        second_part[0][:, :, None] * first_part[1] + second_part[1],
    )


def recurrence(query_pre, input_pre, forward_pre, backward_pre, forget_gap, log_decay, rec_gain):
    heads_local = log_decay.shape[2]
    row_count = query_pre.shape[0]

    def to_heads(tensor):
        return tensor.astype(jnp.float32).reshape(row_count, heads_local, -1).transpose(1, 0, 2)

    def gate_terms(pre_act, gap_row, decay_row):
        closing = jax.nn.sigmoid(-to_heads(pre_act)) * gap_row.reshape(heads_local, 1, -1)
        return (closing, jnp.log1p(-closing) + decay_row[:, :, None])

    queries = jax.nn.silu(to_heads(query_pre)) * KD ** (-0.5)
    values = to_heads(input_pre)
    keys_fwd, gate_fwd = gate_terms(forward_pre, forget_gap[0], log_decay[0, 0])
    keys_bwd, gate_bwd = gate_terms(backward_pre, forget_gap[1], log_decay[0, 1])
    identity = (
        jnp.ones((heads_local, KD), jnp.float32),
        jnp.zeros((heads_local, KD, VD), jnp.float32),
    )
    local_fwd, decayed_fwd, offset_fwd, state_fwd = block_pass(queries, keys_fwd, values, gate_fwd)
    incoming_fwd = entering((jnp.exp(offset_fwd), state_fwd), "sp", chain_combine, identity, False)
    forward = local_fwd + jnp.einsum("htd,hde->hte", decayed_fwd, incoming_fwd[1], precision=HIGH)
    local_bwd, decayed_bwd, offset_bwd, state_bwd = block_pass(
        jnp.flip(queries, 1), jnp.flip(keys_bwd, 1), jnp.flip(values, 1), jnp.flip(gate_bwd, 1)
    )
    incoming_bwd = entering((jnp.exp(offset_bwd), state_bwd), "sp", chain_combine, identity, True)
    backward = jnp.flip(
        local_bwd + jnp.einsum("htd,hde->hte", decayed_bwd, incoming_bwd[1], precision=HIGH), 1
    )
    joined = forward + backward
    joined = joined * lax.rsqrt(jnp.mean(joined * joined, axis=-1, keepdims=True) + EPS)
    joined = joined * rec_gain.reshape(heads_local, 1, VD)
    return joined.transpose(1, 0, 2).reshape(row_count, heads_local * VD).astype(jnp.bfloat16)


def convolve(conv_pre, glu_pre, conv_kernel, conv_gain):
    gated = (conv_pre.astype(jnp.float32) * jax.nn.sigmoid(glu_pre.astype(jnp.float32))).astype(
        jnp.bfloat16
    )
    half_width = conv_kernel.shape[0] // 2
    padded = padded_2(gated, (("sp", 0),), half_width)
    convolved = lax.conv_general_dilated(
        padded.astype(jnp.float32)[None],
        conv_kernel.astype(jnp.float32)[:, None, :],
        (1,),
        "VALID",
        dimension_numbers=("NWC", "WIO", "NWC"),
        feature_group_count=gated.shape[1],
        precision=HIGH,
    )[0]
    totals = lax.psum((jnp.sum(convolved, axis=-1), jnp.sum(convolved * convolved, axis=-1)), "tp")
    full_width = convolved.shape[1] * lax.axis_size("tp")
    mean_c = (totals[0] / full_width)[:, None]
    variance = (totals[1] / full_width)[:, None] - mean_c * mean_c
    return jax.nn.silu((convolved - mean_c) * lax.rsqrt(variance + EPS) * conv_gain).astype(
        jnp.bfloat16
    )


def body(
    tokens,
    norm_gain,
    rec_query,
    rec_input,
    rec_forward,
    rec_backward,
    forget_gap,
    log_decay,
    rec_gain,
    conv_value,
    conv_gate,
    conv_kernel,
    conv_gain,
    out_rec,
    out_conv,
):
    row_values = tokens[0].astype(jnp.float32)
    normed = row_values * lax.rsqrt(jnp.mean(row_values * row_values, axis=-1, keepdims=True) + EPS)
    normed = (normed * norm_gain).astype(jnp.bfloat16)
    whole = lax.all_gather(normed, "tp", axis=0, tiled=True)
    row_count = whole.shape[0]
    pieces = (
        lax.all_gather(rec_query, "sp", axis=0, tiled=True),
        lax.all_gather(rec_input, "sp", axis=0, tiled=True),
        lax.all_gather(rec_forward, "sp", axis=0, tiled=True),
        lax.all_gather(rec_backward, "sp", axis=0, tiled=True),
        lax.all_gather(conv_value, "sp", axis=0, tiled=True),
        lax.all_gather(conv_gate, "sp", axis=0, tiled=True),
    )
    results = tuple(
        (
            jnp.dot(whole, weight_piece, preferred_element_type=jnp.float32)
            for weight_piece in pieces
        )
    )
    projected = tuple((result.astype(jnp.bfloat16) for result in results))
    rec_out = recurrence(
        projected[0], projected[1], projected[2], projected[3], forget_gap, log_decay, rec_gain
    )
    conv_out = convolve(projected[4], projected[5], conv_kernel, conv_gain)
    both_out = jnp.concatenate([rec_out, conv_out], axis=1)
    out_local = jnp.concatenate([out_rec, out_conv], axis=0)
    full_columns = lax.all_gather(out_local, "sp", axis=1, tiled=True)
    own_rows = row_count // lax.axis_size("tp")
    rows_part = lax.slice_in_dim(both_out, 0, own_rows * lax.axis_size("tp"), axis=0)
    mixed = lax.psum_scatter(
        jnp.dot(rows_part, full_columns, preferred_element_type=jnp.float32).astype(jnp.bfloat16),
        "tp",
        scatter_dimension=0,
        tiled=True,
    )
    return mixed[None]


MESH = pl.DeviceIdType.MESH
PACK = 8


def dot_as(a, b, ca, cb, precision=HIGH):
    return lax.dot_general(
        a, b, (((ca,), (cb,)), ((), ())), precision=precision, preferred_element_type=jnp.float32
    )


def fused_kernel(
    n, nf, hl, tokens_in, gain_in, w0, w1, w2, w3, w4, w5, decay_in, gap_in,
    rgain_in, cgain_in, taps_in, out_r, out_c, o_ref, decay_v, gap_v, rgain_v, cgain_v, taps_v,
    tokens, gain, pack,    x, wbuf, ow, pk, ld, dec, proj, accf, accb, gp, yout, yall, mo, fin, st,
    w_send, w_recv, x_send, x_recv, t_send, t_recv, d_send, p_send, p_recv, l_send, l_recv,
    o_send, o_recv, a_send, a_recv, f_send, f_recv, s_send, s_recv, loc, ini,
):
    s = lax.axis_index("sp")
    f = lax.axis_index("fs")
    t = lax.axis_index("tp")
    other = 1 - t
    rows = tokens.shape[1]
    width = KD
    weights = (w0, w1, w2, w3, w4, w5)
    kslice = w0.shape[0]
    krows = kslice // nf
    half = out_r.shape[0]
    groups = n * width

    def at(sp=s, fs=f, tp=t):
        return {"sp": sp, "fs": fs, "tp": tp}

    def remote(src, dst, send, recv, to):
        return pltpu.make_async_remote_copy(
            src_ref=src, dst_ref=dst, send_sem=send, recv_sem=recv, device_id=to,
            device_id_type=MESH,
        )

    entry = [
        pltpu.make_async_copy(src, dst, ini.at[i])
        for i, (src, dst) in enumerate(
            (
                (tokens_in, tokens), (gain_in, gain), (decay_in, decay_v), (gap_in, gap_v),
                (rgain_in, rgain_v), (cgain_in, cgain_v), (taps_in, taps_v),
            )
        )
    ]
    for copy in entry:
        copy.start()

    barrier = pltpu.get_barrier_semaphore()
    for d in range(n):
        for c in range(2):
            if d or c:
                pl.semaphore_signal(
                    barrier, inc=1, device_id=at(sp=lax.rem(s + d, n), tp=lax.rem(t + c, 2)),
                    device_id_type=MESH,
                )
    for d in range(1, nf):
        pl.semaphore_signal(
            barrier, inc=1, device_id=at(fs=lax.rem(f + d, nf)), device_id_type=MESH
        )
    pl.semaphore_wait(barrier, 2 * n - 1 + nf - 1)

    def wrows(place, quarter):
        return pl.ds(pl.multiple_of(place * kslice + quarter * krows, krows), krows)

    def wcols(core):
        return pl.ds(0, (4 - 2 * core) * width)

    def whole(place):
        return pl.ds(pl.multiple_of(place * kslice, kslice), kslice)

    mine = pl.ds(pl.multiple_of(f * krows, krows), krows)
    for j in range(hl):
        to_s = t * hl + j
        cols = pl.ds(j * width, width)
        for core in range(2):
            for at_m, m in enumerate((0, 1, 2, 3) if core == 0 else (4, 5)):
                at_cols = pl.ds(at_m * width, width)
                src = weights[m].at[:, cols]
                dst = wbuf.at[whole(s), at_cols]

                @pl.when((to_s == s) & (t == core))
                def _(src=src, dst=dst):
                    pltpu.make_async_copy(src, dst, w_recv.at[s]).start()

                @pl.when((to_s == s) & (t != core))
                def _(src=src, dst=dst, core=core, j=j):
                    remote(src, dst, w_send.at[j, core], w_recv.at[s], at(tp=core)).start()

                @pl.when(to_s != s)
                def _(m=m, cols=cols, at_cols=at_cols, core=core, to_s=to_s, j=j):
                    remote(
                        weights[m].at[mine, cols], wbuf.at[wrows(s, f), at_cols],
                        w_send.at[j, core], w_recv.at[s], at(sp=to_s, tp=core),
                    ).start()

    for copy in entry[2:]:
        copy.wait()
    taps_n = taps_v.shape[0]
    for j in range(hl):
        cols = slice(j * width, (j + 1) * width)
        pack[j, 0:2, :] = decay_v[0, :, j, :]
        pack[j, 2:4, :] = gap_v[:, cols]
        pack[j, 4:5, :] = rgain_v[:, cols]
        pack[j, 5:6, :] = cgain_v[:, cols]
        pack[j, 6:PACK, :] = jnp.zeros((PACK - 6, width), jnp.float32)
        pack[j, PACK : PACK + taps_n, :] = taps_v[:, cols].astype(jnp.float32)
    entry[0].wait()
    entry[1].wait()
    values = tokens[0].astype(jnp.float32)
    normed = values * lax.rsqrt(jnp.mean(values * values, axis=-1, keepdims=True) + EPS)

    def slot(place, core):
        return pl.ds(pl.multiple_of(place * 2 * rows + core * rows, rows), rows)

    x[slot(s, t), :] = (normed * gain[...]).astype(jnp.bfloat16)

    def token(place, core, send, to):
        part = x.at[slot(place, core)]
        return remote(part, part, send, t_recv.at[place, core], to)

    def token_right(place):
        return token(place, t, t_send.at[place, 0], at(sp=lax.rem(s + 1, n)))

    def token_left(place):
        return token(place, t, t_send.at[place, 1], at(sp=lax.rem(s + n - 1, n)))

    def token_partner(place):
        return token(place, t, d_send.at[place], at(tp=other))

    @pl.when(s < n - 1)
    def _():
        token_right(s).start()

    @pl.when(s > 0)
    def _():
        token_left(s).start()

    token_partner(s).start()

    for j in range(hl):
        to_s = t * hl + j
        here0 = (to_s == s) & (t == 0)
        src = pack.at[j, pl.ds(0, PACK)]

        @pl.when(here0)
        def _(src=src):
            pltpu.make_async_copy(src, ld.at[s], l_recv.at[s]).start()

        @pl.when(jnp.logical_not(here0))
        def _(src=src, j=j, to_s=to_s):
            remote(src, ld.at[s], l_send.at[j], l_recv.at[s], at(sp=to_s, tp=0)).start()

        @pl.when(to_s == s)
        def _(j=j):
            pltpu.make_async_copy(pack.at[j], pk, p_recv).start()
            remote(pack.at[j], pk, p_send, p_recv, at(tp=other)).start()

    own_out = []
    for which, ref in enumerate((out_r, out_c)):
        part = ow.at[pl.ds(pl.multiple_of(which * groups + t * half, half), half)]
        own_out.append(remote(ref, part, o_send.at[which], o_recv.at[which], at(tp=other)))
        own_out[-1].start()
        pltpu.make_async_copy(ref, part, loc.at[which]).start()

    def share(core, place, d):
        part = wbuf.at[wrows(place, f), wcols(core)]
        return remote(
            part, part, x_send.at[place, d], x_recv.at[place, f], at(fs=lax.rem(f + d, nf))
        )

    for core in range(2):

        @pl.when(t == core)
        def _(core=core):
            for e in range(1, n):
                place = lax.rem(s + e, n)
                part = wbuf.at[wrows(place, f), wcols(core)]
                pltpu.make_async_copy(part, part, w_recv.at[place]).wait()
                for d in range(1, nf):
                    share(core, place, d).start()

    for d in range(1, n):

        @pl.when(s >= d)
        def _(d=d):
            place = s - d
            token_right(place).wait_recv()
            token_partner(place).start()

            @pl.when(s < n - 1)
            def _():
                token_right(place).start()

        @pl.when(s + d < n)
        def _(d=d):
            place = s + d
            token_left(place).wait_recv()
            token_partner(place).start()

            @pl.when(s > 0)
            def _():
                token_left(place).start()

    for place in range(n):
        part = x.at[slot(place, other)]
        remote(part, part, d_send.at[place], t_recv.at[place, other], at(tp=other)).wait_recv()
    for core in range(2):

        @pl.when(t == core)
        def _(core=core):
            part = wbuf.at[whole(s), wcols(core)]
            pltpu.make_async_copy(part, part, w_recv.at[s]).wait()
            for e in range(1, n):
                place = lax.rem(s + e, n)
                for d in range(1, nf):
                    quarter = lax.rem(f + d, nf)
                    part = wbuf.at[wrows(place, quarter), wcols(core)]
                    remote(
                        part, part, x_send.at[place, d], x_recv.at[place, quarter], at(fs=quarter)
                    ).wait_recv()

    pltpu.make_async_copy(pk, pk, p_recv).wait()

    total = x.shape[0]
    chunk = min(256, total)

    def project(core):
        @pl.loop(0, total // chunk)
        def _(i):
            at_rows = pl.ds(pl.multiple_of(i * chunk, chunk), chunk)
            proj[at_rows, wcols(core)] = jnp.dot(
                x[at_rows, :], wbuf[:, wcols(core)], preferred_element_type=jnp.float32
            ).astype(jnp.bfloat16)

    def send_all(core, to_s, to_t):
        dst = yall.at[:, pl.ds(pl.multiple_of(core * groups + s * width, width), width)]
        return remote(
            yout.at[to_t], dst, a_send.at[to_s, to_t], a_recv.at[s, core], at(sp=to_s, tp=to_t)
        )

    def spread(core):
        for d in range(n):
            for c in range(2):
                if d or c:
                    send_all(core, lax.rem(s + n - d, n), (core + c) % 2).start()
        dst = yall.at[:, pl.ds(pl.multiple_of(core * groups + s * width, width), width)]
        pltpu.make_async_copy(yout.at[core], dst, a_recv.at[s, core]).start()

    def spread_wait(core):
        for d in range(n):
            for c in range(2):
                if d or c:
                    send_all(core, lax.rem(s + n - d, n), (core + c) % 2).wait_send()

    @pl.when(t == 0)
    def _():
        project(0)
        for place in range(n):
            pltpu.make_async_copy(ld.at[place], ld.at[place], l_recv.at[place]).wait()
        pick = lax.broadcasted_iota(jnp.int32, (PACK, width), 0)
        span = 2 * rows
        for place in range(n):
            for d in range(2):
                dec[d, pl.ds(place * span, span), :] = dot_as(
                    ld[place], (pick == d).astype(jnp.float32), 0, 0
                )
        row_i = lax.broadcasted_iota(jnp.int32, (BLOCK, BLOCK), 0)
        col_i = lax.broadcasted_iota(jnp.int32, (BLOCK, BLOCK), 1)
        masks = (row_i >= col_i, row_i <= col_i)
        blocks = total // BLOCK

        def one(d, p, state):
            at_rows = pl.ds(pl.multiple_of(p * BLOCK, BLOCK), BLOCK)
            qp = proj[at_rows, 0:width].astype(jnp.float32)
            query = qp * jax.nn.sigmoid(qp) * width ** (-0.5)
            value = proj[at_rows, width : 2 * width].astype(jnp.float32)
            pre = proj[at_rows, (2 + d) * width : (3 + d) * width].astype(jnp.float32)
            keys = pk[2 + d : 3 + d, :] * jax.nn.sigmoid(-pre)
            gate = jnp.log1p(-keys) + dec[d, at_rows, :]
            cum = dot_as(masks[d].astype(jnp.float32), gate, 1, 0)
            query_g = query * jnp.exp(cum)
            key_g = keys * jnp.exp(-cum)
            scores = jnp.where(masks[d], dot_as(query_g, key_g, 1, 1), 0.0)
            result = dot_as(scores, value, 1, 0) + dot_as(query_g, state, 1, 1)
            last = cum[BLOCK - 1 : BLOCK, :] if d == 0 else cum[0:1, :]
            weighted = keys * jnp.exp(last - cum)
            state = state * jnp.exp(last) + dot_as(value, weighted, 0, 0)
            (accf, accb)[d][at_rows, :] = result
            return state

        def step(i, states):
            return one(0, i, states[0]), one(1, blocks - 1 - i, states[1])

        zero = jnp.zeros((width, width), jnp.float32)
        lax.fori_loop(0, blocks, step, (zero, zero))
        for place in range(n):
            for c in range(2):
                at_rows = pl.ds((place * 2 + c) * rows, rows)
                joined = accf[at_rows, :] + accb[at_rows, :]
                joined = joined * lax.rsqrt(
                    jnp.mean(joined * joined, axis=-1, keepdims=True) + EPS
                )
                yout[c, pl.ds(place * rows, rows), :] = (joined * pk[4:5, :]).astype(jnp.bfloat16)
        spread(0)

    @pl.when(t == 1)
    def _():
        project(1)
        taps = pk.shape[0] - PACK
        pad = 16
        gp[0:pad, :] = jnp.zeros((pad, width), jnp.float32)
        gp[pad + total : 2 * pad + total, :] = jnp.zeros((pad, width), jnp.float32)
        value = proj[:, 0:width].astype(jnp.float32)
        gate = proj[:, width : 2 * width].astype(jnp.float32)
        gp[pad : pad + total, :] = (
            (value * jax.nn.sigmoid(gate)).astype(jnp.bfloat16).astype(jnp.float32)
        )
        first = pad - taps_half(taps)

        for b in range(total // rows):
            acc = jnp.zeros((rows, width), jnp.float32)
            for j in range(taps):
                acc = acc + pk[PACK + j : PACK + j + 1, :] * gp[pl.ds(b * rows + first + j, rows), :]
            accf[pl.ds(b * rows, rows), :] = acc
        conv = accf[...]
        ones = jnp.ones((8, width), jnp.float32)
        st[s, 0] = dot_as(ones, conv, 1, 1)
        st[s, 1] = dot_as(ones, conv * conv, 1, 1)

        def stat(d):
            return remote(
                st.at[s], st.at[s], s_send.at[d], s_recv.at[s], at(sp=lax.rem(s + d, n))
            )

        for d in range(1, n):
            stat(d).start()
        for d in range(1, n):
            place = lax.rem(s + d, n)
            remote(st.at[place], st.at[place], s_send.at[d], s_recv.at[place], at(sp=place)).wait_recv()
        stats = st[0]
        for place in range(1, n):
            stats = stats + st[place]
        stats = stats / groups
        mean_r = stats[0]
        inv_r = lax.rsqrt(stats[1] - mean_r * mean_r + EPS)
        eighth = jnp.full((8, width), 0.125, jnp.float32)
        mean_c = dot_as(mean_r, eighth, 0, 0)
        inv_c = dot_as(inv_r, eighth, 0, 0)
        out = (accf[...] - mean_c) * inv_c * pk[5:6, :]
        out = (out * jax.nn.sigmoid(out)).astype(jnp.bfloat16)
        for place in range(n):
            for c in range(2):
                b = (place * 2 + c) * rows
                yout[c, pl.ds(place * rows, rows), :] = out[b : b + rows]
        spread(1)
        for d in range(1, n):
            stat(d).wait_send()

    for which, ref in enumerate((out_r, out_c)):
        part = ow.at[pl.ds(pl.multiple_of(which * groups + t * half, half), half)]
        pltpu.make_async_copy(ref, part, loc.at[which]).wait()
        part = ow.at[pl.ds(pl.multiple_of(which * groups + other * half, half), half)]
        remote(ref, part, o_send.at[which], o_recv.at[which], at(tp=other)).wait_recv()
    for core in range(2):
        for place in range(n):
            part = yall.at[:, pl.ds(core * groups + place * width, width)]
            pltpu.make_async_copy(part, part, a_recv.at[place, core]).wait()
    result = jnp.dot(yall[...], ow[...], preferred_element_type=jnp.float32)
    mo[...] = result.astype(jnp.bfloat16)
    cols = out_r.shape[1]
    fin_cols = pl.ds(pl.multiple_of(s * cols, cols), cols)

    def give(to_s):
        return remote(
            mo.at[pl.ds(pl.multiple_of(to_s * rows, rows), rows)], fin.at[:, fin_cols],
            f_send.at[to_s], f_recv.at[s], at(sp=to_s),
        )

    for d in range(1, n):
        give(lax.rem(s + d, n)).start()
    o_ref[0, :, fin_cols] = mo[pl.ds(pl.multiple_of(s * rows, rows), rows), :]
    for d in range(1, n):
        place = lax.rem(s + d, n)
        part_cols = pl.ds(pl.multiple_of(place * cols, cols), cols)
        remote(
            mo.at[pl.ds(0, rows)], fin.at[:, part_cols], f_send.at[place], f_recv.at[place],
            at(sp=place),
        ).wait_recv()
        o_ref[0, :, part_cols] = fin[:, part_cols]

    for core in range(2):

        @pl.when(t == core)
        def _(core=core):
            spread_wait(core)
            for e in range(1, n):
                for d in range(1, nf):
                    share(core, lax.rem(s + e, n), d).wait_send()

    for d in range(1, n):
        give(lax.rem(s + d, n)).wait_send()
    for copy in own_out:
        copy.wait_send()
    for j in range(hl):
        to_s = t * hl + j
        for core in range(2):

            @pl.when((to_s == s) & (t != core))
            def _(j=j, core=core):
                part = wbuf.at[whole(s), wcols(core)]
                remote(part, part, w_send.at[j, core], w_recv.at[s], at(tp=core)).wait_send()

            @pl.when(to_s != s)
            def _(j=j, core=core, to_s=to_s):
                part = wbuf.at[wrows(s, f), wcols(core)]
                remote(
                    part, part, w_send.at[j, core], w_recv.at[s], at(sp=to_s, tp=core)
                ).wait_send()

        @pl.when(jnp.logical_not((to_s == s) & (t == 0)))
        def _(j=j, to_s=to_s):
            remote(
                pack.at[j, pl.ds(0, PACK)], ld.at[s], l_send.at[j], l_recv.at[s],
                at(sp=to_s, tp=0),
            ).wait_send()

        @pl.when(to_s == s)
        def _(j=j):
            remote(pack.at[j], pk, p_send, p_recv, at(tp=other)).wait_send()

    for place in range(n):
        token_partner(place).wait_send()

        @pl.when((place <= s) & (s < n - 1))
        def _(place=place):
            token_right(place).wait_send()

        @pl.when((place >= s) & (s > 0))
        def _(place=place):
            token_left(place).wait_send()


def taps_half(taps):
    return taps // 2


def fused_body(
    n, nf, tokens, norm_gain, rec_query, rec_input, rec_forward, rec_backward, forget_gap,
    log_decay, rec_gain, conv_value, conv_gate, conv_kernel, conv_gain, out_rec, out_conv,
):
    hl = log_decay.shape[2]
    rows, d = tokens.shape[1:]
    total = 2 * rows * n
    taps = conv_kernel.shape[0]
    width = KD
    groups = n * width
    cols = out_rec.shape[1]

    vmem = pl.BlockSpec(memory_space=pltpu.VMEM)
    bf, f32 = jnp.bfloat16, jnp.float32
    dma = pltpu.SemaphoreType.DMA
    small = (log_decay, forget_gap, rec_gain[None], conv_gain[None], conv_kernel)
    scratch = [
        *(pltpu.VMEM(a.shape, a.dtype) for a in small),
        pltpu.VMEM(tokens.shape, bf),
        pltpu.VMEM((1, d), f32),
        pltpu.VMEM((hl, PACK + taps, width), f32),
        pltpu.VMEM((total, d), bf),
        pltpu.VMEM((d, 4 * width), bf),
        pltpu.VMEM((2 * groups, cols), bf),
        pltpu.VMEM((PACK + taps, width), f32),
        pltpu.VMEM((n, PACK, width), f32),
        pltpu.VMEM((2, total, width), f32),
        pltpu.VMEM((total, 4 * width), bf),
        pltpu.VMEM((total, width), f32),
        pltpu.VMEM((total, width), f32),
        pltpu.VMEM((total + 32, width), f32),
        pltpu.VMEM((2, total // 2, width), bf),
        pltpu.VMEM((total // 2, 2 * groups), bf),
        pltpu.VMEM((total // 2, cols), bf),
        pltpu.VMEM((rows, d), bf),
        pltpu.VMEM((n, 2, 8, total), f32),
        dma((hl, 2)), dma((n,)),
        dma((n, nf)), dma((n, nf)),
        dma((n, 2)), dma((n, 2)), dma((n,)),
        dma(()), dma(()),
        dma((hl,)), dma((n,)),
        dma((2,)), dma((2,)),
        dma((n, 2)), dma((n, 2)),
        dma((n,)), dma((n,)),
        dma((n,)), dma((n,)),
        dma((2,)), dma((7,)),
    ]
    return pl.pallas_call(
        functools.partial(fused_kernel, n, nf, hl),
        out_shape=jax.ShapeDtypeStruct((1, rows, d), bf),
        in_specs=[pl.BlockSpec(memory_space=pl.ANY)] * 15,
        out_specs=vmem,
        scratch_shapes=scratch,
        compiler_params=pltpu.CompilerParams(
            collective_id=0, has_side_effects=True, vmem_limit_bytes=60 * 1024 * 1024
        ),
    )(
        tokens, norm_gain[None], rec_query, rec_input, rec_forward, rec_backward, conv_value,
        conv_gate, *small, out_rec, out_conv,
    )


def fits(n, nf, nt, tokens, rec_query, log_decay, conv_value, conv_kernel, out_rec):
    heads = log_decay.shape[2]
    rows = tokens.shape[1] // (n * nt)
    return (
        nt == 2
        and n == heads
        and tokens.shape[0] == nf
        and rec_query.shape[1] == heads * KD
        and conv_value.shape[1] == heads * VD
        and KD == VD
        and 2 * rows == KD
        and rec_query.shape[0] % (n * nf * 16) == 0
        and conv_kernel.shape[0] // 2 <= 15
    )


def layer(mesh, *args):
    n, nf, nt = (mesh.shape[a] for a in ("sp", "fs", "tp"))
    fast = fits(n, nf, nt, args[0], args[2], args[7], args[9], args[11], args[13])
    return sharded(mesh, functools.partial(fused_body, n, nf) if fast else body)(*args)


def solution(mesh):
    return functools.partial(layer, mesh)


def sharded(mesh, body):
    return jax.shard_map(
        body,
        mesh=mesh,
        in_specs=(
            P("fs", ("sp", "tp"), None),
            P(),
            P("sp", "tp"),
            P("sp", "tp"),
            P("sp", "tp"),
            P("sp", "tp"),
            P(None, "tp"),
            P("fs", None, "tp", "sp"),
            P("tp"),
            P("sp", "tp"),
            P("sp", "tp"),
            P(None, "tp"),
            P("tp"),
            P("tp", "sp"),
            P("tp", "sp"),
        ),
        out_specs=P("fs", ("sp", "tp"), None),
        check_vma=False,
    )
```

profile of v0, /device:TPU:0, one launch (start us, length us, event | category | flops | bytes accessed | tf_op | source)
XLA Modules:
  0.0 61.9 jit_solution(12840744761778568382)
XLA Ops:
  0.0 60.2 %shard_map.145 = bf16[1,64,2048]{2,1,0:T(8,128)(2,1)} custom-call(bf16[1,64,2048]{2,1,0:T(8,128)(2,1)} %tokens_in.1, f32[1,2048]{1,0:T(1,128)} %bitcast.3, bf16[512,256]{1,0:T(8,128)(2,1)} %w0.1, bf16[512,256]{1,0:T(8,128)(2,1)} %w1.1, bf16[512,256]{1,0:T(8,128)(2,1)} %w2.1, bf16[512,256]{1,0:T(8,128)(2,1)} %w3.1, bf16[512,256]{1,0:T(8,128)(2,1)} %w4.1, ...), custom_call_target="tpu_custom_call" | custom-call | tf_op jit(solution)/shard_map/pallas_call | solution.py:719
  60.2 1.7 %copy.17 = bf16[1,64,2048]{2,1,0:T(8,128)(2,1)} copy(bf16[1,64,2048]{2,1,0:T(8,128)(2,1)} %shard_map.145) | data formatting | bytes 524288
where the time goes:
time: 62.8 us; the launch traced here: 61.9 us
  Pallas kernels  60.2 us (96%)
  local copies, waits for them, and re-layouts  1.67 us (3%)
    pallas_call x1, Pallas kernels, fused_body(): pl.pallas_call(functools.partial(fused_kernel, n, nf, hl), out_shape=jax....  60.2 us
    unnamed x1, local copies, waits for them, and re-layouts  1.67 us

commit v1 on v0

v1 whole, which is shorter than its diff:
```python
import functools

import jax
import jax.numpy as jnp
from jax import lax
from jax.experimental import pallas as pl
from jax.experimental.pallas import tpu as pltpu
from jax.sharding import PartitionSpec as P

KD = 128
VD = 128
BLOCK = 64


EPS = 1e-06
HIGH = lax.Precision.HIGHEST


def entering(x, axis, join, neutral, backward):
    count = lax.axis_size(axis)
    place = lax.axis_index(axis)
    ahead = count - 1 - place if backward else place
    gathered = jax.tree.map(
        lambda a, kind: lax.all_gather(a.astype(kind), axis), x, (jnp.bfloat16, jnp.bfloat16)
    )
    state = jax.tree.map(lambda a, e: jnp.zeros_like(a) + jnp.asarray(e, a.dtype), x, neutral)

    def one(lap, state):
        source = count - 1 - lap if backward else lap
        return join(
            state,
            jax.tree.map(
                lambda a, own: lax.dynamic_index_in_dim(a, source, 0, False).astype(own.dtype),
                gathered,
                x,
            ),
        )

    return lax.fori_loop(0, ahead, one, state)


def padded_2(cells, sides, width):
    for axis, dim in sides:
        count = lax.axis_size(axis)
        ends = count - 1
        head = lax.slice_in_dim(cells, 0, width, axis=dim)
        tail = lax.slice_in_dim(cells, cells.shape[dim] - width, cells.shape[dim], axis=dim)
        cells = jnp.concatenate(
            [
                lax.ppermute(tail, axis, [(i, (i + 1) % count) for i in range(ends)]),
                cells,
                lax.ppermute(head, axis, [((i + 1) % count, i) for i in range(ends)]),
            ],
            axis=dim,
        )
    return cells


def block_pass(queries, key_rows, value_rows, log_gate):
    heads_n, length_n, key_dim = queries.shape
    value_dim = value_rows.shape[-1]
    blocks = length_n // BLOCK

    def split_blocks(tensor):
        return tensor.reshape(heads_n, blocks, BLOCK, tensor.shape[-1]).transpose(1, 0, 2, 3)

    def join_blocks(tensor):
        return tensor.transpose(1, 0, 2, 3).reshape(heads_n, length_n, tensor.shape[-1])

    lower_mask = jnp.tril(jnp.ones((BLOCK, BLOCK), bool))

    def advance(carried, inputs):
        states, offset = carried
        query_b, key_b, value_b, gate_b = inputs
        cumulative = jnp.cumsum(gate_b, axis=1)
        query_g = query_b * jnp.exp(cumulative)
        key_g = key_b * jnp.exp(-cumulative)
        scores = jnp.einsum("htd,hsd->hts", query_g, key_g, precision=HIGH)
        scores = jnp.where(lower_mask, scores, 0.0)
        result = jnp.einsum("hts,hse->hte", scores, value_b, precision=HIGH)
        result = result + jnp.einsum("htd,hde->hte", query_g, states, precision=HIGH)
        last_g = cumulative[:, -1, :]
        weighted = key_b * jnp.exp(last_g[:, None, :] - cumulative)
        states = jnp.exp(last_g)[:, :, None] * states + jnp.einsum(
            "hsd,hse->hde", weighted, value_b, precision=HIGH
        )
        decayed = query_b * jnp.exp(offset[:, None, :] + cumulative)
        return ((states, offset + last_g), (result, decayed))

    start_state = jnp.zeros((heads_n, key_dim, value_dim), jnp.float32)
    start_offset = jnp.zeros((heads_n, key_dim), jnp.float32)
    inputs = (
        split_blocks(queries),
        split_blocks(key_rows),
        split_blocks(value_rows),
        split_blocks(log_gate),
    )
    final_pair, outputs = lax.scan(advance, (start_state, start_offset), inputs)
    return (join_blocks(outputs[0]), join_blocks(outputs[1]), final_pair[1], final_pair[0])


def chain_combine(first_part, second_part):
    return (
        first_part[0] * second_part[0],
        second_part[0][:, :, None] * first_part[1] + second_part[1],
    )


def recurrence(query_pre, input_pre, forward_pre, backward_pre, forget_gap, log_decay, rec_gain):
    heads_local = log_decay.shape[2]
    row_count = query_pre.shape[0]

    def to_heads(tensor):
        return tensor.astype(jnp.float32).reshape(row_count, heads_local, -1).transpose(1, 0, 2)

    def gate_terms(pre_act, gap_row, decay_row):
        closing = jax.nn.sigmoid(-to_heads(pre_act)) * gap_row.reshape(heads_local, 1, -1)
        return (closing, jnp.log1p(-closing) + decay_row[:, :, None])

    queries = jax.nn.silu(to_heads(query_pre)) * KD ** (-0.5)
    values = to_heads(input_pre)
    keys_fwd, gate_fwd = gate_terms(forward_pre, forget_gap[0], log_decay[0, 0])
    keys_bwd, gate_bwd = gate_terms(backward_pre, forget_gap[1], log_decay[0, 1])
    identity = (
        jnp.ones((heads_local, KD), jnp.float32),
        jnp.zeros((heads_local, KD, VD), jnp.float32),
    )
    local_fwd, decayed_fwd, offset_fwd, state_fwd = block_pass(queries, keys_fwd, values, gate_fwd)
    incoming_fwd = entering((jnp.exp(offset_fwd), state_fwd), "sp", chain_combine, identity, False)
    forward = local_fwd + jnp.einsum("htd,hde->hte", decayed_fwd, incoming_fwd[1], precision=HIGH)
    local_bwd, decayed_bwd, offset_bwd, state_bwd = block_pass(
        jnp.flip(queries, 1), jnp.flip(keys_bwd, 1), jnp.flip(values, 1), jnp.flip(gate_bwd, 1)
    )
    incoming_bwd = entering((jnp.exp(offset_bwd), state_bwd), "sp", chain_combine, identity, True)
    backward = jnp.flip(
        local_bwd + jnp.einsum("htd,hde->hte", decayed_bwd, incoming_bwd[1], precision=HIGH), 1
    )
    joined = forward + backward
    joined = joined * lax.rsqrt(jnp.mean(joined * joined, axis=-1, keepdims=True) + EPS)
    joined = joined * rec_gain.reshape(heads_local, 1, VD)
    return joined.transpose(1, 0, 2).reshape(row_count, heads_local * VD).astype(jnp.bfloat16)


def convolve(conv_pre, glu_pre, conv_kernel, conv_gain):
    gated = (conv_pre.astype(jnp.float32) * jax.nn.sigmoid(glu_pre.astype(jnp.float32))).astype(
        jnp.bfloat16
    )
    half_width = conv_kernel.shape[0] // 2
    padded = padded_2(gated, (("sp", 0),), half_width)
    convolved = lax.conv_general_dilated(
        padded.astype(jnp.float32)[None],
        conv_kernel.astype(jnp.float32)[:, None, :],
        (1,),
        "VALID",
        dimension_numbers=("NWC", "WIO", "NWC"),
        feature_group_count=gated.shape[1],
        precision=HIGH,
    )[0]
    totals = lax.psum((jnp.sum(convolved, axis=-1), jnp.sum(convolved * convolved, axis=-1)), "tp")
    full_width = convolved.shape[1] * lax.axis_size("tp")
    mean_c = (totals[0] / full_width)[:, None]
    variance = (totals[1] / full_width)[:, None] - mean_c * mean_c
    return jax.nn.silu((convolved - mean_c) * lax.rsqrt(variance + EPS) * conv_gain).astype(
        jnp.bfloat16
    )


def body(
    tokens,
    norm_gain,
    rec_query,
    rec_input,
    rec_forward,
    rec_backward,
    forget_gap,
    log_decay,
    rec_gain,
    conv_value,
    conv_gate,
    conv_kernel,
    conv_gain,
    out_rec,
    out_conv,
):
    row_values = tokens[0].astype(jnp.float32)
    normed = row_values * lax.rsqrt(jnp.mean(row_values * row_values, axis=-1, keepdims=True) + EPS)
    normed = (normed * norm_gain).astype(jnp.bfloat16)
    whole = lax.all_gather(normed, "tp", axis=0, tiled=True)
    row_count = whole.shape[0]
    pieces = (
        lax.all_gather(rec_query, "sp", axis=0, tiled=True),
        lax.all_gather(rec_input, "sp", axis=0, tiled=True),
        lax.all_gather(rec_forward, "sp", axis=0, tiled=True),
        lax.all_gather(rec_backward, "sp", axis=0, tiled=True),
        lax.all_gather(conv_value, "sp", axis=0, tiled=True),
        lax.all_gather(conv_gate, "sp", axis=0, tiled=True),
    )
    results = tuple(
        (
            jnp.dot(whole, weight_piece, preferred_element_type=jnp.float32)
            for weight_piece in pieces
        )
    )
    projected = tuple((result.astype(jnp.bfloat16) for result in results))
    rec_out = recurrence(
        projected[0], projected[1], projected[2], projected[3], forget_gap, log_decay, rec_gain
    )
    conv_out = convolve(projected[4], projected[5], conv_kernel, conv_gain)
    both_out = jnp.concatenate([rec_out, conv_out], axis=1)
    out_local = jnp.concatenate([out_rec, out_conv], axis=0)
    full_columns = lax.all_gather(out_local, "sp", axis=1, tiled=True)
    own_rows = row_count // lax.axis_size("tp")
    rows_part = lax.slice_in_dim(both_out, 0, own_rows * lax.axis_size("tp"), axis=0)
    mixed = lax.psum_scatter(
        jnp.dot(rows_part, full_columns, preferred_element_type=jnp.float32).astype(jnp.bfloat16),
        "tp",
        scatter_dimension=0,
        tiled=True,
    )
    return mixed[None]


MESH = pl.DeviceIdType.MESH
PACK = 8


def dot_as(a, b, ca, cb, precision=HIGH):
    return lax.dot_general(
        a, b, (((ca,), (cb,)), ((), ())), precision=precision, preferred_element_type=jnp.float32
    )


PIECES = (2, 4)
TSUB = 2
LAG = 4
OUTS = 4
(
    PARAMS, DECAY, _, TOKENS, TOKENS_ON, WEIGHTS, OWN, ACROSS, BESIDE, OUT_OWN, OUT, OUT_ACROSS,
    OUT_BESIDE, GIVE, HALO, STATE, STATS, MIXED, GROUPS,
) = range(19)


def pair_kernel(
    tokens_in, gain_in, w0, w1, w2, w3, w4, w5, decay_in, gap_in, rgain_in, cgain_in, taps_in,
    out_r, out_c, o_ref, decay_v, gap_v, rgain_v, cgain_v, taps_v, tokens, gain,
    xs, x, wbuf, ow, pack, pk, lds, ld, dec, proj, gp, halo_s, halo_r, st_s, st_in, cacc, stat,
    yout, ya, mo, fin, ini, snd, w_own, w_recv, y_recv, d_recv, t_recv, p_recv, l_recv, h_recv,
    s_recv, c_recv, a_recv, o_own, o_recv, q_recv, g_recv, f_recv,
):
    s = lax.axis_index("sp")
    f = lax.axis_index("fs")
    t = lax.axis_index("tp")
    other = 1 - t
    col = lax.rem(f, 2)
    row = f // 2
    part = s // 2
    pair = lax.rem(s, 2)
    near = s + 1 - 2 * pair
    far = lax.rem(s + 2, 4)
    cross = 3 - s
    fx = f + 1 - 2 * col
    fy = lax.rem(f + 2, 4)
    fd = 3 - f
    head = 2 * pair + col
    rows = tokens.shape[1]
    span = 2 * rows
    total = 2 * span
    width = KD
    weights = (w0, w1, w2, w3, w4, w5)
    kslice = w0.shape[0]
    fourth = kslice // 4
    kinds = (range(4, 6), range(0, 4))
    half = out_r.shape[0]
    quarter = half // 4
    cols = out_r.shape[1]
    groups = 4 * width
    ways = (near, 2 - part, 3 - 3 * part)
    NEAR, INNER, OUTER = range(3)
    mine = OUTER - (pair - part) * (pair - part)
    own_col = t == col
    own_weights = t == pair

    def at(sp=s, fs=f, tp=t):
        return {"sp": sp, "fs": fs, "tp": tp}

    def remote(src, dst, send, recv, to):
        return pltpu.make_async_remote_copy(
            src_ref=src, dst_ref=dst, send_sem=send, recv_sem=recv, device_id=to,
            device_id_type=MESH,
        )

    def when(cond, act):
        if cond is None:
            act()
        else:
            pl.when(cond)(act)

    def send(src, dst, group, recv, to, cond=None):
        when(cond, remote(src, dst, snd.at[group], recv, to).start)

    def arrived(ref, sem, cond=None):
        when(cond, pltpu.make_async_copy(ref, ref, sem).wait)

    def aligned(start, size, unit):
        return pl.ds(pl.multiple_of(start, unit), size)

    entry = [
        pltpu.make_async_copy(src, dst, ini.at[i])
        for i, (src, dst) in enumerate(
            (
                (tokens_in, tokens), (gain_in, gain), (decay_in, decay_v), (gap_in, gap_v),
                (rgain_in, rgain_v), (cgain_in, cgain_v), (taps_in, taps_v),
            )
        )
    ]
    for copy in entry:
        copy.start()

    def slot(place, core, k=None):
        if k is None:
            return aligned(place * span + core * rows, rows, rows)
        step = rows // TSUB
        return aligned(place * span + core * rows + k * step, step, step)

    barrier = pltpu.get_barrier_semaphore()
    greet = [at(sp=lax.rem(s + d, 4), tp=lax.rem(t + c, 2)) for d in range(4) for c in range(2) if d or c]
    greet += [at(sp=z, fs=fx, tp=lax.rem(t + c, 2)) for z in (s, near) for c in range(2)]
    greet += [at(fs=fy), at(fs=fd)]
    for to in greet:
        pl.semaphore_signal(barrier, inc=1, device_id=to, device_id_type=MESH)

    for copy in entry:
        copy.wait()
    values = tokens[0].astype(jnp.float32)
    normed = values * lax.rsqrt(jnp.mean(values * values, axis=-1, keepdims=True) + EPS)
    normed = (normed * gain[...]).astype(jnp.bfloat16)
    xs[...] = normed

    @pl.when(own_col)
    def _():
        x[slot(pair, t), :] = normed

    taps_n = taps_v.shape[0]
    at_col = aligned(col * width, width, width)
    pack[0:2, :] = gap_v[:, at_col]
    pack[2:3, :] = rgain_v[:, at_col]
    pack[3:4, :] = cgain_v[:, at_col]
    pack[4:PACK, :] = jnp.zeros((PACK - 4, width), jnp.float32)
    pack[PACK : PACK + taps_n, :] = taps_v[:, at_col].astype(jnp.float32)
    for j in range(2):
        lds[j, 0:2, :] = decay_v[0, :, j, :]
        lds[j, 2:PACK, :] = jnp.zeros((PACK - 2, span), jnp.float32)
    pl.semaphore_wait(barrier, len(greet))

    def piece(kind, place, side, core, i):
        size = fourth // PIECES[kind]
        at_cols = pl.ds(kinds[kind].start * width, len(kinds[kind]) * width)
        return wbuf.at[
            aligned(place * kslice + (side * 2 + core) * fourth + i * size, size, size), at_cols
        ]

    def flag(kind, way, i):
        return (PIECES[0] * 3 if kind else 0) + way * PIECES[kind] + i

    def send_weights(kind, i):
        size = fourth // PIECES[kind]
        for place, way in ((far, mine), (cross, mine), (near, NEAR)):
            for core in range(2):
                src_rows = aligned((row * 2 + core) * fourth + i * size, size, size)
                dst_rows = aligned(s * kslice + (row * 2 + core) * fourth + i * size, size, size)
                for m in kinds[kind]:
                    send(
                        weights[m].at[src_rows, at_col],
                        wbuf.at[dst_rows, pl.ds(m * width, width)],
                        WEIGHTS, w_recv.at[flag(kind, way, i)], at(sp=place, tp=core),
                        own_weights if place is far else jnp.logical_not(own_weights),
                    )

    @pl.when(own_weights)
    def _():
        pk[...] = pack[...]

    send(pack, pk, PARAMS, p_recv, at(tp=other), own_weights)
    for j in range(2):
        to = at(sp=2 * part + t, fs=2 * row + j, tp=col)
        here = own_weights & (col == j) & own_col

        @pl.when(here)
        def _(j=j):
            pltpu.make_async_copy(lds.at[j], ld.at[pair], l_recv.at[pair]).start()

        send(lds.at[j], ld.at[pair], DECAY + j, l_recv.at[pair], to, jnp.logical_not(here))

    def send_tokens(k):
        step = rows // TSUB
        src = xs.at[pl.ds(k * step, step)]
        dst = x.at[slot(pair, t, k)]
        sem = t_recv.at[pair, t, k]
        send(src, dst, TOKENS, sem, at(sp=near, tp=col))
        send(src, dst, TOKENS, sem, at(fs=fx, tp=col))
        send(src, dst, TOKENS_ON, sem, at(tp=col), jnp.logical_not(own_col))

    own_rows = aligned(s * kslice, kslice, kslice)
    for m in range(6):

        @pl.when(own_weights)
        def _(m=m):
            src = weights[m].at[:, at_col]
            dst = wbuf.at[own_rows, pl.ds(m * width, width)]
            kind = 0 if m in kinds[0] else 1
            remote(src, dst, snd.at[OWN], w_own.at[kind], at(tp=other)).start()
            pltpu.make_async_copy(src, dst, w_own.at[kind]).start()

    def out_cols(place):
        return aligned(place * cols, cols, cols)

    for which, ref in enumerate((out_r, out_c)):
        dst = ow.at[which, aligned(t * half, half, half), pl.ds(0, cols)]
        pltpu.make_async_copy(ref, dst, o_own.at[0]).start()
        send(ref, dst, OUT_OWN, o_own.at[1], at(tp=other))

    def relay_tokens(k):
        scope(f"T{k}")
        for core in range(2):
            ref = x.at[slot(1 - pair, core, k)]
            arrived(ref, t_recv.at[1 - pair, core, k], own_col)
            send(ref, ref, TOKENS_ON, t_recv.at[1 - pair, core, k], at(fs=fx), own_col)

    def first_hop(kind, way, i):
        scope(f"A{kind}{way}{i}")
        ref = piece(kind, ways[way], row, t, i)
        arrived(ref, w_recv.at[flag(kind, way, i)])
        send(ref, ref, ACROSS, y_recv.at[flag(kind, way, i)], at(fs=fy))
        send(ref, ref, BESIDE, d_recv.at[kind], at(tp=other))

    def second_hop(kind, way, i):
        scope(f"B{kind}{way}{i}")
        ref = piece(kind, ways[way], 1 - row, t, i)
        arrived(ref, y_recv.at[flag(kind, way, i)])
        send(ref, ref, BESIDE, d_recv.at[kind], at(tp=other))

    def weights_wait(kind):
        at_cols = pl.ds(kinds[kind].start * width, len(kinds[kind]) * width)
        arrived(wbuf.at[own_rows, at_cols], w_own.at[kind])
        arrived(wbuf.at[pl.ds(0, 6 * fourth), at_cols], d_recv.at[kind])

    cut = quarter // (OUTS // 2)

    def out_part(core, quart, k):
        return ow.at[
            k // (OUTS // 2),
            aligned(core * half + quart * quarter + k % (OUTS // 2) * cut, cut, cut),
            pl.ds(cols, cols),
        ]

    def send_out(k):
        src = (out_r, out_c)[k // (OUTS // 2)].at[
            aligned(f * quarter + k % (OUTS // 2) * cut, cut, cut), :
        ]
        send(src, out_part(t, f, k), OUT, o_recv.at[k], at(sp=far))

    def out_first(k):
        scope(f"X{k}")
        ref = out_part(t, f, k)
        arrived(ref, o_recv.at[k])
        send(ref, ref, OUT_ACROSS, q_recv.at[k, 0], at(fs=fx))
        send(ref, ref, OUT_ACROSS, q_recv.at[k, 1], at(fs=fy))
        send(ref, ref, OUT_BESIDE, g_recv, at(tp=other))

    def out_second(k):
        scope(f"Y{k}")
        for j, (source, to) in enumerate(((fx, fy), (fy, fx))):
            ref = out_part(t, source, k)
            arrived(ref, q_recv.at[k, j])
            if k % 2 == j:
                send(ref, ref, OUT_ACROSS, q_recv.at[k, 2], at(fs=to))
            send(ref, ref, OUT_BESIDE, g_recv, at(tp=other))

    def out_third(k):
        scope(f"Z{k}")
        ref = out_part(t, fd, k)
        arrived(ref, q_recv.at[k, 2])
        send(ref, ref, OUT_BESIDE, g_recv, at(tp=other))

    def run(step, *pieces):
        for k in pieces:
            step(k)

    def project(n0):
        at_n = pl.ds(n0 * 2 * width, 2 * width)
        proj[:, at_n] = jnp.dot(
            x[...], wbuf[:, at_n], preferred_element_type=jnp.float32
        ).astype(jnp.bfloat16)

    for k in range(TSUB):
        send_tokens(k)
    for kind in range(2):
        for i in range(PIECES[kind]):
            send_weights(kind, i)
    bf = jnp.bfloat16
    blocks = total // BLOCK
    pad = 16

    def decay_columns():
        scope("dec")
        for place in range(2):
            arrived(ld.at[place], l_recv.at[place])
        arrived(pk, p_recv, jnp.logical_not(own_weights))
        pick = lax.broadcasted_iota(jnp.int32, (PACK, width), 0)
        for place in range(2):
            for d in range(2):
                dec[d, pl.ds(place * span, span), :] = dot_as(
                    ld[place], (pick == d).astype(jnp.float32), 0, 0
                )

    def conv_open():
        scope("tokwait")
        for k in range(TSUB):
            for place in (pair, 1 - pair):
                for core in range(2):
                    local = own_col & (place == pair) & (t == core)
                    done = own_col & (place == 1 - pair)
                    skip = local | done if place is not pair else local
                    arrived(x.at[slot(place, core, k)], t_recv.at[place, core, k], jnp.logical_not(skip))
        scope("cwait")
        weights_wait(0)
        scope("projectc")
        project(2)
        scope("gate")
        conv_pre = proj[:, 4 * width : 5 * width].astype(jnp.float32)
        glu_pre = proj[:, 5 * width : 6 * width].astype(jnp.float32)
        gated = (conv_pre * jax.nn.sigmoid(glu_pre)).astype(jnp.bfloat16)
        gp[pad : pad + total, :] = gated.astype(jnp.float32)
        halo_s[...] = jnp.where(part == 0, gated[total - pad :], gated[0:pad])
        send(halo_s, halo_r, HALO, h_recv, at(sp=far))
        for k in range(OUTS):
            send_out(k)

    def conv_close():
        scope("conv")
        arrived(halo_r, h_recv)
        halo = halo_r[...].astype(jnp.float32)
        none = jnp.zeros((pad, width), jnp.float32)
        gp[0:pad, :] = jnp.where(part == 1, halo, none)
        gp[pad + total : 2 * pad + total, :] = jnp.where(part == 0, halo, none)
        first = pad - taps_n // 2
        for b in range(blocks):
            acc = jnp.zeros((BLOCK, width), jnp.float32)
            for j in range(taps_n):
                acc = acc + pk[PACK + j : PACK + j + 1, :] * gp[pl.ds(b * BLOCK + first + j, BLOCK), :]
            cacc[pl.ds(b * BLOCK, BLOCK), :] = acc
        conv = cacc[...]
        ones = jnp.ones((8, width), jnp.float32)
        stat[head, 0] = dot_as(ones, conv, 1, 1)
        stat[head, 1] = dot_as(ones, conv * conv, 1, 1)
        own_stat = stat.at[head]
        send(own_stat, own_stat, STATS, c_recv, at(fs=fx))
        send(own_stat, own_stat, STATS, c_recv, at(sp=near))
        send(own_stat, own_stat, STATS, c_recv, at(sp=near, fs=fx))

    order = [
        (0, INNER, 0), (0, INNER, 1), (1, INNER, 0), (0, OUTER, 0), (0, NEAR, 0), (0, OUTER, 1),
        (0, NEAR, 1), (1, INNER, 1), (1, OUTER, 0), (1, NEAR, 0), (1, INNER, 2), (1, OUTER, 1),
        (1, NEAR, 1), (1, INNER, 3), (1, OUTER, 2), (1, NEAR, 2), (1, OUTER, 3), (1, NEAR, 3),
    ]
    for k, hop in enumerate(order):
        if k == 2:
            relay_tokens(0)
        if k == 3:
            relay_tokens(1)
        first_hop(*hop)
        if k >= LAG:
            second_hop(*order[k - LAG])
        if k == 5:
            decay_columns()
        if k == 7 + LAG:
            conv_open()
    run(out_first, 0, 1)
    conv_close()
    for hop in order[-LAG:]:
        second_hop(*hop)
    run(out_first, 2, 3)
    scope("rwait")
    weights_wait(1)
    scope("projectr")
    project(1)
    project(0)
    scope("states")
    def f32(n0):
        return proj[:, n0 * width : (n0 + 1) * width].astype(jnp.float32)

    query_pre = f32(0)
    query = query_pre * jax.nn.sigmoid(query_pre) * width ** (-0.5)
    value = proj[:, width : 2 * width]
    keys, gates = [], []
    for d in range(2):
        key = pk[d : d + 1, :] * jax.nn.sigmoid(-f32(2 + d))
        keys.append(key)
        gates.append(jnp.log1p(-key) + dec[d])
    row_i = lax.broadcasted_iota(jnp.int32, (total, total), 0)
    col_i = lax.broadcasted_iota(jnp.int32, (total, total), 1)
    same = (row_i // BLOCK) == (col_i // BLOCK)
    lower = same & (row_i >= col_i)
    upper = same & (row_i <= col_i)
    both = jnp.concatenate(gates, axis=1)
    high = both.astype(bf)
    low = (both - high.astype(jnp.float32)).astype(bf)
    tri = lower.astype(jnp.float32).astype(bf)
    sums = jnp.dot(tri, high, preferred_element_type=jnp.float32) + jnp.dot(
        tri, low, preferred_element_type=jnp.float32
    )
    lasts = [sums[b * BLOCK + BLOCK - 1 : (b + 1) * BLOCK, :] for b in range(blocks)]

    def spread_rows(parts):
        return jnp.concatenate([jnp.broadcast_to(a, (BLOCK, width)) for a in parts], axis=0)

    last = [[a[:, d * width : (d + 1) * width] for a in lasts] for d in range(2)]
    last_rows = [spread_rows(last[d]) for d in range(2)]
    cum_f = sums[:, 0:width]
    cum_b = last_rows[1] - sums[:, width:] + gates[1]
    cums = (cum_f, cum_b)
    query_g = [(query * jnp.exp(cums[d])).astype(bf) for d in range(2)]
    key_g = [(keys[d] * jnp.exp(-cums[d])).astype(bf) for d in range(2)]
    weighted = jnp.concatenate(
        [(keys[d] * jnp.exp(last_rows[d] - cums[d])).astype(bf) for d in range(2)], axis=1
    )
    outer = [
        lax.dot_general(
            value[b * BLOCK : (b + 1) * BLOCK], weighted[b * BLOCK : (b + 1) * BLOCK],
            (((0,), (0,)), ((), ())), preferred_element_type=jnp.float32,
        )
        for b in range(blocks)
    ]
    states = [[None] * blocks, [None] * blocks]
    ends, offsets = [], [[None] * blocks, [None] * blocks]
    for d in range(2):
        state = jnp.zeros((width, width), jnp.float32)
        offset = jnp.zeros((1, width), jnp.float32)
        for b in range(blocks) if d == 0 else range(blocks - 1, -1, -1):
            states[d][b] = state
            offsets[d][b] = offset
            state = state * jnp.exp(last[d][b]) + outer[b][:, d * width : (d + 1) * width]
            offset = offset + last[d][b]
        ends.append(state)
    st_s[...] = jnp.where(part == 0, ends[0], ends[1]).astype(bf)
    send(st_s, st_in, STATE, s_recv, at(sp=far))


    run(out_second, 0, 1)
    scope("scores")
    scores = [
        lax.dot_general(
            query_g[d], key_g[d], (((1,), (1,)), ((), ())), preferred_element_type=jnp.float32
        )
        for d in range(2)
    ]
    scores = (jnp.where(lower, scores[0], 0.0) + jnp.where(upper, scores[1], 0.0)).astype(bf)
    inner = jnp.dot(scores, value, preferred_element_type=jnp.float32)
    carried = jnp.concatenate(
        [
            lax.dot_general(
                jnp.concatenate([q[b * BLOCK : (b + 1) * BLOCK] for q in query_g], axis=1),
                jnp.concatenate([states[d][b].astype(bf) for d in range(2)], axis=1),
                (((1,), (1,)), ((), ())), preferred_element_type=jnp.float32,
            )
            for b in range(blocks)
        ],
        axis=0,
    )
    reach = jnp.where(
        part == 1, spread_rows(offsets[0]) + cum_f, spread_rows(offsets[1]) + cum_b
    )
    query_in = (query * jnp.exp(reach)).astype(bf)
    def mix(which, out):
        for core in range(2):
            for place in range(2):
                at_row = place * span + core * rows
                yout[which, pl.ds(core * span + place * rows, rows), :] = out[
                    at_row : at_row + rows
                ].astype(bf)
        dst = ya.at[:, aligned(which * groups + head * width, width, width)]
        for place in range(2):
            for core in range(2):
                src = yout.at[which, pl.ds(core * span, span)]
                here = own_col & (pair == place) & (t == core)

                @pl.when(here)
                def _(src=src):
                    pltpu.make_async_copy(src, dst, a_recv.at[which]).start()

                send(
                    src, dst, MIXED, a_recv.at[which],
                    at(sp=2 * part + place, fs=2 * row + t, tp=core), jnp.logical_not(here),
                )

    scope("statx")
    arrived(stat.at[pl.ds(0, 3)], c_recv)
    scope("cnorm")
    stats = (stat[0] + stat[1] + stat[2] + stat[3]) / groups
    mean_r = stats[0]
    inv_r = lax.rsqrt(stats[1] - mean_r * mean_r + EPS)
    eighth = jnp.full((8, width), 0.125, jnp.float32)
    mean_c = dot_as(mean_r, eighth, 0, 0)
    inv_c = dot_as(inv_r, eighth, 0, 0)
    out = (cacc[...] - mean_c) * inv_c * pk[3:4, :]
    mix(1, out * jax.nn.sigmoid(out))

    run(out_second, 2, 3)
    scope("statein")
    arrived(st_in, s_recv)
    scope("recnorm")
    joined = inner + carried + lax.dot_general(
        query_in, st_in[...], (((1,), (1,)), ((), ())), preferred_element_type=jnp.float32
    )
    joined = joined * lax.rsqrt(jnp.mean(joined * joined, axis=-1, keepdims=True) + EPS)
    mix(0, joined * pk[2:3, :])

    run(out_third, 0, 1, 2, 3)
    scope("ywait1")
    arrived(ya.at[:, pl.ds(0, groups)], a_recv.at[1])
    for k in range(2):
        arrived(ow.at[:, pl.ds(0, half), pl.ds(0, cols)], o_own.at[k])
    scope("ywait0")
    arrived(ya.at[:, pl.ds(0, groups)], a_recv.at[0])
    near_rows = aligned((1 - pair) * rows, rows, rows)
    for k in range(2):
        scope(f"outmm{k}")
        if k == 1:
            arrived(ow.at[:, pl.ds(0, half), pl.ds(0, cols)], g_recv)
        at_n = pl.ds(k * cols, cols)
        acc = jnp.dot(ya[:, 0:groups], ow[0, :, at_n], preferred_element_type=jnp.float32)
        acc = acc + jnp.dot(ya[:, groups:], ow[1, :, at_n], preferred_element_type=jnp.float32)
        mo[:, at_n] = acc.astype(bf)
        send(mo.at[near_rows, at_n], fin.at[:, at_n], GIVE, f_recv.at[k], at(sp=near))
    own_rows = aligned(pair * rows, rows, rows)
    for k, place in enumerate((s, far)):
        o_ref[0, :, out_cols(place)] = mo[own_rows, pl.ds(k * cols, cols)]
    for k, place in enumerate((near, cross)):
        scope(f"give{k}")
        at_n = pl.ds(k * cols, cols)
        arrived(fin.at[:, at_n], f_recv.at[k])
        o_ref[0, :, out_cols(place)] = fin[:, at_n]

    scope("sendwaits")
    other_weights = jnp.logical_not(own_weights)
    other_col = jnp.logical_not(own_col)
    arrived(pack, snd.at[PARAMS], own_weights)
    for j in range(2):
        here = own_weights & (col == j) & own_col
        arrived(lds.at[j], snd.at[DECAY + j], jnp.logical_not(here))
    arrived(x.at[pl.ds(0, 2 * rows)], snd.at[TOKENS])
    arrived(x.at[pl.ds(0, 2 * rows)], snd.at[TOKENS_ON], own_col)
    arrived(x.at[pl.ds(0, rows)], snd.at[TOKENS_ON], other_col)
    arrived(wbuf.at[pl.ds(0, 2 * fourth)], snd.at[WEIGHTS], own_weights)
    arrived(wbuf.at[pl.ds(0, 4 * fourth)], snd.at[WEIGHTS], other_weights)
    arrived(wbuf.at[pl.ds(0, kslice)], snd.at[OWN], own_weights)
    arrived(wbuf.at[pl.ds(0, 3 * fourth)], snd.at[ACROSS])
    arrived(wbuf.at[pl.ds(0, 6 * fourth)], snd.at[BESIDE])
    arrived(ow.at[:, pl.ds(0, half), pl.ds(0, cols)], snd.at[OUT_OWN])
    arrived(ow.at[:, pl.ds(0, quarter), pl.ds(0, cols)], snd.at[OUT])
    arrived(ow.at[:, pl.ds(0, 3 * quarter), pl.ds(0, cols)], snd.at[OUT_ACROSS])
    arrived(ow.at[:, pl.ds(0, 4 * quarter), pl.ds(0, cols)], snd.at[OUT_BESIDE])
    arrived(halo_s, snd.at[HALO])
    arrived(st_s, snd.at[STATE])
    arrived(stat.at[pl.ds(0, 3)], snd.at[STATS])
    arrived(x.at[pl.ds(0, 6 * span * width // x.shape[1])], snd.at[MIXED], own_col)
    arrived(x.at[pl.ds(0, 8 * span * width // x.shape[1])], snd.at[MIXED], other_col)
    arrived(fin, snd.at[GIVE])
    scope(None)


def scope(name):
    pass


def pair_body(
    tokens, norm_gain, rec_query, rec_input, rec_forward, rec_backward, forget_gap,
    log_decay, rec_gain, conv_value, conv_gate, conv_kernel, conv_gain, out_rec, out_conv,
):
    rows, d = tokens.shape[1:]
    total = 4 * rows
    taps = conv_kernel.shape[0]
    width = KD
    half, cols = out_rec.shape

    bf, f32 = jnp.bfloat16, jnp.float32
    dma = pltpu.SemaphoreType.DMA
    small = (log_decay, forget_gap, rec_gain[None], conv_gain[None], conv_kernel)
    scratch = [
        *(pltpu.VMEM(a.shape, a.dtype) for a in small),
        pltpu.VMEM(tokens.shape, bf),
        pltpu.VMEM((1, d), f32),
        pltpu.VMEM((rows, d), bf),
        pltpu.VMEM((total, d), bf),
        pltpu.VMEM((d, 6 * width), bf),
        pltpu.VMEM((2, 2 * half, 2 * cols), bf),
        pltpu.VMEM((PACK + taps, width), f32),
        pltpu.VMEM((PACK + taps, width), f32),
        pltpu.VMEM((2, PACK, 2 * rows), f32),
        pltpu.VMEM((2, PACK, 2 * rows), f32),
        pltpu.VMEM((2, total, width), f32),
        pltpu.VMEM((total, 6 * width), bf),
        pltpu.VMEM((total + 32, width), f32),
        pltpu.VMEM((16, width), bf),
        pltpu.VMEM((16, width), bf),
        pltpu.VMEM((width, width), bf),
        pltpu.VMEM((width, width), bf),
        pltpu.VMEM((total, width), f32),
        pltpu.VMEM((4, 2, 8, total), f32),
        pltpu.VMEM((2, total, width), bf),
        pltpu.VMEM((2 * rows, 8 * width), bf),
        pltpu.VMEM((2 * rows, 2 * cols), bf),
        pltpu.VMEM((rows, 2 * cols), bf),
        dma((7,)), dma((GROUPS,)), dma((2,)), dma((3 * sum(PIECES),)), dma((3 * sum(PIECES),)),
        dma((2,)), dma((2, 2, TSUB)), dma(()), dma((2,)), dma(()),
        dma(()), dma(()), dma((2,)), dma((2,)), dma((OUTS,)), dma((OUTS, 3)), dma(()), dma((2,)),
    ]
    return pl.pallas_call(
        pair_kernel,
        out_shape=jax.ShapeDtypeStruct((1, rows, d), bf),
        in_specs=[pl.BlockSpec(memory_space=pl.ANY)] * 15,
        out_specs=pl.BlockSpec(memory_space=pltpu.VMEM),
        scratch_shapes=scratch,
        compiler_params=pltpu.CompilerParams(
            collective_id=0, has_side_effects=True, vmem_limit_bytes=60 * 1024 * 1024
        ),
    )(
        tokens, norm_gain[None], rec_query, rec_input, rec_forward, rec_backward, conv_value,
        conv_gate, *small, out_rec, out_conv,
    )


def fits(n, nf, nt, tokens, rec_query, log_decay, conv_value, conv_kernel, out_rec):
    heads = log_decay.shape[2]
    rows = tokens.shape[1] // (n * nt)
    return (
        nt == 2
        and n == 4
        and nf == 4
        and n == heads
        and tokens.shape[0] == nf
        and rec_query.shape[1] == heads * KD
        and conv_value.shape[1] == heads * VD
        and KD == VD
        and 2 * rows == KD
        and rows % (16 * TSUB) == 0
        and rec_query.shape[0] % (n * 4 * max(PIECES) * 16) == 0
        and out_rec.shape[0] % (nt * nf * 16) == 0
        and conv_kernel.shape[0] // 2 <= 15
    )


def layer(mesh, *args):
    n, nf, nt = (mesh.shape[a] for a in ("sp", "fs", "tp"))
    fast = fits(n, nf, nt, args[0], args[2], args[7], args[9], args[11], args[13])
    return sharded(mesh, pair_body if fast else body)(*args)


def solution(mesh):
    return functools.partial(layer, mesh)


def sharded(mesh, body):
    return jax.shard_map(
        body,
        mesh=mesh,
        in_specs=(
            P("fs", ("sp", "tp"), None),
            P(),
            P("sp", "tp"),
            P("sp", "tp"),
            P("sp", "tp"),
            P("sp", "tp"),
            P(None, "tp"),
            P("fs", None, "tp", "sp"),
            P("tp"),
            P("sp", "tp"),
            P("sp", "tp"),
            P(None, "tp"),
            P("tp"),
            P("tp", "sp"),
            P("tp", "sp"),
        ),
        out_specs=P("fs", ("sp", "tp"), None),
        check_vma=False,
    )
```

time: 62.8 us -> 49.3 us (0.79); the launches traced: 61.9 us -> 49.1 us
  Pallas kernels: 60.2 us -> 47.4 us
    pallas_call x1, Pallas kernels: 60.2 us -> 47.4 us  [pair_body(): pl.pallas_call(pair_kernel, out_shape=jax.ShapeDtypeStruct((1, rows, d),...]
where the time goes in v1:
time: 49.3 us; the launch traced here: 49.1 us
  Pallas kernels  47.4 us (96%)
  local copies, waits for them, and re-layouts  1.67 us (3%)
    pallas_call x1, Pallas kernels, pair_body(): pl.pallas_call(pair_kernel, out_shape=jax.ShapeDtypeStruct((1, rows, d),...  47.4 us
    unnamed x1, local copies, waits for them, and re-layouts  1.67 us

profile of v1, /device:TPU:0, one launch (start us, length us, event | category | flops | bytes accessed | tf_op | source)
XLA Modules:
  0.0 49.1 jit_solution(13861502997527897896)
XLA Ops:
  0.0 47.4 %shard_map.145 = bf16[1,64,2048]{2,1,0:T(8,128)(2,1)} custom-call(bf16[1,64,2048]{2,1,0:T(8,128)(2,1)} %tokens_in.1, f32[1,2048]{1,0:T(1,128)} %bitcast.3, bf16[512,256]{1,0:T(8,128)(2,1)} %w0.1, bf16[512,256]{1,0:T(8,128)(2,1)} %w1.1, bf16[512,256]{1,0:T(8,128)(2,1)} %w2.1, bf16[512,256]{1,0:T(8,128)(2,1)} %w3.1, bf16[512,256]{1,0:T(8,128)(2,1)} %w4.1, ...), custom_call_target="tpu_custom_call" | custom-call | tf_op jit(solution)/shard_map/pallas_call | solution.py:818
  47.4 1.7 %copy.17 = bf16[1,64,2048]{2,1,0:T(8,128)(2,1)} copy(bf16[1,64,2048]{2,1,0:T(8,128)(2,1)} %shard_map.145) | data formatting | bytes 524288

commit v2 on v1

--- a/solution.py
+++ b/solution.py
@@ -230,9 +230,9 @@
     )
 
 
-PIECES = (2, 4)
+PIECES = (2, 4, 1)
 TSUB = 2
-LAG = 4
+LAG = 6
 OUTS = 4
 (
     PARAMS, DECAY, _, TOKENS, TOKENS_ON, WEIGHTS, OWN, ACROSS, BESIDE, OUT_OWN, OUT, OUT_ACROSS,
@@ -269,7 +269,7 @@
     weights = (w0, w1, w2, w3, w4, w5)
     kslice = w0.shape[0]
     fourth = kslice // 4
-    kinds = (range(4, 6), range(0, 4))
+    kinds = (range(4, 6), range(1, 4), range(0, 1))
     half = out_r.shape[0]
     quarter = half // 4
     cols = out_r.shape[1]
@@ -360,7 +360,7 @@
         ]
 
     def flag(kind, way, i):
-        return (PIECES[0] * 3 if kind else 0) + way * PIECES[kind] + i
+        return 3 * sum(PIECES[:kind]) + way * PIECES[kind] + i
 
     def send_weights(kind, i):
         size = fourth // PIECES[kind]
@@ -407,7 +407,7 @@
         def _(m=m):
             src = weights[m].at[:, at_col]
             dst = wbuf.at[own_rows, pl.ds(m * width, width)]
-            kind = 0 if m in kinds[0] else 1
+            kind = [m in k for k in kinds].index(True)
             remote(src, dst, snd.at[OWN], w_own.at[kind], at(tp=other)).start()
             pltpu.make_async_copy(src, dst, w_own.at[kind]).start()
 
@@ -472,7 +472,7 @@
         for j, (source, to) in enumerate(((fx, fy), (fy, fx))):
             ref = out_part(t, source, k)
             arrived(ref, q_recv.at[k, j])
-            if k % 2 == j:
+            if j == 0:
                 send(ref, ref, OUT_ACROSS, q_recv.at[k, 2], at(fs=to))
             send(ref, ref, OUT_BESIDE, g_recv, at(tp=other))
 
@@ -486,15 +486,16 @@
         for k in pieces:
             step(k)
 
-    def project(n0):
-        at_n = pl.ds(n0 * 2 * width, 2 * width)
-        proj[:, at_n] = jnp.dot(
-            x[...], wbuf[:, at_n], preferred_element_type=jnp.float32
+    def project(kind):
+        at_cols = pl.ds(kinds[kind].start * width, len(kinds[kind]) * width)
+        proj[:, at_cols] = jnp.dot(
+            x[...], wbuf[:, at_cols], preferred_element_type=jnp.float32
         ).astype(jnp.bfloat16)
 
     for k in range(TSUB):
+        send_weights(0, k)
         send_tokens(k)
-    for kind in range(2):
+    for kind in range(1, 3):
         for i in range(PIECES[kind]):
             send_weights(kind, i)
     bf = jnp.bfloat16
@@ -525,7 +526,7 @@
         scope("cwait")
         weights_wait(0)
         scope("projectc")
-        project(2)
+        project(0)
         scope("gate")
         conv_pre = proj[:, 4 * width : 5 * width].astype(jnp.float32)
         glu_pre = proj[:, 5 * width : 6 * width].astype(jnp.float32)
@@ -559,14 +560,15 @@
         send(own_stat, own_stat, STATS, c_recv, at(sp=near, fs=fx))
 
     order = [
-        (0, INNER, 0), (0, INNER, 1), (1, INNER, 0), (0, OUTER, 0), (0, NEAR, 0), (0, OUTER, 1),
-        (0, NEAR, 1), (1, INNER, 1), (1, OUTER, 0), (1, NEAR, 0), (1, INNER, 2), (1, OUTER, 1),
-        (1, NEAR, 1), (1, INNER, 3), (1, OUTER, 2), (1, NEAR, 2), (1, OUTER, 3), (1, NEAR, 3),
+        (0, INNER, 0), (0, NEAR, 0), (0, INNER, 1), (1, INNER, 0), (0, OUTER, 0), (0, NEAR, 1),
+        (1, INNER, 1), (0, OUTER, 1), (1, INNER, 2), (1, OUTER, 0), (1, NEAR, 0), (1, INNER, 3),
+        (1, OUTER, 1), (1, NEAR, 1), (1, OUTER, 2), (1, NEAR, 2), (1, OUTER, 3), (1, NEAR, 3),
+        (2, INNER, 0), (2, OUTER, 0), (2, NEAR, 0),
     ]
     for k, hop in enumerate(order):
-        if k == 2:
+        if k == 4:
             relay_tokens(0)
-        if k == 3:
+        if k == 7:
             relay_tokens(1)
         first_hop(*hop)
         if k >= LAG:
@@ -575,22 +577,18 @@
             decay_columns()
         if k == 7 + LAG:
             conv_open()
-    run(out_first, 0, 1)
     conv_close()
-    for hop in order[-LAG:]:
+    for hop in order[-LAG:-3]:
         second_hop(*hop)
-    run(out_first, 2, 3)
-    scope("rwait")
+    scope("kwait")
     weights_wait(1)
-    scope("projectr")
+    scope("projectk")
     project(1)
-    project(0)
+
     scope("states")
     def f32(n0):
         return proj[:, n0 * width : (n0 + 1) * width].astype(jnp.float32)
 
-    query_pre = f32(0)
-    query = query_pre * jax.nn.sigmoid(query_pre) * width ** (-0.5)
     value = proj[:, width : 2 * width]
     keys, gates = [], []
     for d in range(2):
@@ -619,7 +617,6 @@
     cum_f = sums[:, 0:width]
     cum_b = last_rows[1] - sums[:, width:] + gates[1]
     cums = (cum_f, cum_b)
-    query_g = [(query * jnp.exp(cums[d])).astype(bf) for d in range(2)]
     key_g = [(keys[d] * jnp.exp(-cums[d])).astype(bf) for d in range(2)]
     weighted = jnp.concatenate(
         [(keys[d] * jnp.exp(last_rows[d] - cums[d])).astype(bf) for d in range(2)], axis=1
@@ -646,8 +643,17 @@
     send(st_s, st_in, STATE, s_recv, at(sp=far))
 
 
-    run(out_second, 0, 1)
+    for hop in order[-3:]:
+        second_hop(*hop)
+    run(out_first, 0, 1, 2, 3)
+    scope("qwait")
+    weights_wait(2)
+    scope("projectq")
+    project(2)
     scope("scores")
+    query_pre = f32(0)
+    query = query_pre * jax.nn.sigmoid(query_pre) * width ** (-0.5)
+    query_g = [(query * jnp.exp(cums[d])).astype(bf) for d in range(2)]
     scores = [
         lax.dot_general(
             query_g[d], key_g[d], (((1,), (1,)), ((), ())), preferred_element_type=jnp.float32
@@ -679,10 +685,10 @@
                     at_row : at_row + rows
                 ].astype(bf)
         dst = ya.at[:, aligned(which * groups + head * width, width, width)]
-        for place in range(2):
+        for place in (near, s):
             for core in range(2):
                 src = yout.at[which, pl.ds(core * span, span)]
-                here = own_col & (pair == place) & (t == core)
+                here = own_col & (place == s) & (t == core)
 
                 @pl.when(here)
                 def _(src=src):
@@ -690,7 +696,7 @@
 
                 send(
                     src, dst, MIXED, a_recv.at[which],
-                    at(sp=2 * part + place, fs=2 * row + t, tp=core), jnp.logical_not(here),
+                    at(sp=place, fs=2 * row + t, tp=core), jnp.logical_not(here),
                 )
 
     scope("statx")
@@ -705,7 +711,7 @@
     out = (cacc[...] - mean_c) * inv_c * pk[3:4, :]
     mix(1, out * jax.nn.sigmoid(out))
 
-    run(out_second, 2, 3)
+    run(out_second, 0, 1)
     scope("statein")
     arrived(st_in, s_recv)
     scope("recnorm")
@@ -715,6 +721,7 @@
     joined = joined * lax.rsqrt(jnp.mean(joined * joined, axis=-1, keepdims=True) + EPS)
     mix(0, joined * pk[2:3, :])
 
+    run(out_second, 2, 3)
     run(out_third, 0, 1, 2, 3)
     scope("ywait1")
     arrived(ya.at[:, pl.ds(0, groups)], a_recv.at[1])
@@ -811,13 +818,13 @@
         pltpu.VMEM((2 * rows, 8 * width), bf),
         pltpu.VMEM((2 * rows, 2 * cols), bf),
         pltpu.VMEM((rows, 2 * cols), bf),
-        dma((7,)), dma((GROUPS,)), dma((2,)), dma((3 * sum(PIECES),)), dma((3 * sum(PIECES),)),
-        dma((2,)), dma((2, 2, TSUB)), dma(()), dma((2,)), dma(()),
+        dma((7,)), dma((GROUPS,)), dma((3,)), dma((3 * sum(PIECES),)), dma((3 * sum(PIECES),)),
+        dma((3,)), dma((2, 2, TSUB)), dma(()), dma((2,)), dma(()),
         dma(()), dma(()), dma((2,)), dma((2,)), dma((OUTS,)), dma((OUTS, 3)), dma(()), dma((2,)),
     ]
     return pl.pallas_call(
         pair_kernel,
-        out_shape=jax.ShapeDtypeStruct((1, rows, d), bf),
+        out_shape=pltpu.VMEM((1, rows, d), bf),
         in_specs=[pl.BlockSpec(memory_space=pl.ANY)] * 15,
         out_specs=pl.BlockSpec(memory_space=pltpu.VMEM),
         scratch_shapes=scratch,

time: 49.3 us -> 46.6 us (0.945)
  Pallas kernels: 47.4 us -> 45.7 us
  local copies, waits for them, and re-layouts: 1.67 us -> 0.71 us
    pallas_call x1, Pallas kernels: 47.4 us -> 45.7 us  [pair_body(): pl.pallas_call(pair_kernel, out_shape=pltpu.VMEM((1, rows, d), bf), in_sp...]
    unnamed x1, local copies, waits for them, and re-layouts: 1.67 us -> 0.71 us
where the time goes in v2:
time: 46.6 us; the launch traced here: 46.5 us
  Pallas kernels  45.7 us (98%)
  local copies, waits for them, and re-layouts  0.71 us (2%)
    pallas_call x1, Pallas kernels, pair_body(): pl.pallas_call(pair_kernel, out_shape=pltpu.VMEM((1, rows, d), bf), in_sp...  45.7 us

profile of v2, /device:TPU:0, one launch (start us, length us, event | category | flops | bytes accessed | tf_op | source)
XLA Modules:
  0.0 46.5 jit_solution(8811722006396960178)
XLA Ops:
  0.0 45.7 %shard_map.145 = bf16[1,64,2048]{2,1,0:T(8,128)(2,1)S(1)} custom-call(bf16[1,64,2048]{2,1,0:T(8,128)(2,1)} %tokens_in.1, f32[1,2048]{1,0:T(1,128)} %bitcast.3, bf16[512,256]{1,0:T(8,128)(2,1)} %w0.1, bf16[512,256]{1,0:T(8,128)(2,1)} %w1.1, bf16[512,256]{1,0:T(8,128)(2,1)} %w2.1, bf16[512,256]{1,0:T(8,128)(2,1)} %w3.1, bf16[512,256]{1,0:T(8,128)(2,1)} %w4.1, ...), custom_call_target="tpu_custom_call" | custom-call | tf_op jit(solution)/shard_map/pallas_call | solution.py:825
  45.8 0.7 %copy.17 = bf16[1,64,2048]{2,1,0:T(8,128)(2,1)} copy(bf16[1,64,2048]{2,1,0:T(8,128)(2,1)S(1)} %shard_map.145) | data formatting | bytes 524288

commit v3 on v2

--- a/solution.py
+++ b/solution.py
@@ -234,6 +234,7 @@
 TSUB = 2
 LAG = 6
 OUTS = 4
+OUT_AT = 15
 (
     PARAMS, DECAY, _, TOKENS, TOKENS_ON, WEIGHTS, OWN, ACROSS, BESIDE, OUT_OWN, OUT, OUT_ACROSS,
     OUT_BESIDE, GIVE, HALO, STATE, STATS, MIXED, GROUPS,
@@ -534,7 +535,7 @@
         gp[pad : pad + total, :] = gated.astype(jnp.float32)
         halo_s[...] = jnp.where(part == 0, gated[total - pad :], gated[0:pad])
         send(halo_s, halo_r, HALO, h_recv, at(sp=far))
-        for k in range(OUTS):
+        for k in range(OUTS // 2, OUTS):
             send_out(k)
 
     def conv_close():
@@ -575,9 +576,11 @@
             second_hop(*order[k - LAG])
         if k == 5:
             decay_columns()
-        if k == 7 + LAG:
+        if k == OUT_AT:
+            for early in range(OUTS // 2):
+                send_out(early)
+        if k == 17:
             conv_open()
-    conv_close()
     for hop in order[-LAG:-3]:
         second_hop(*hop)
     scope("kwait")
@@ -645,7 +648,8 @@
 
     for hop in order[-3:]:
         second_hop(*hop)
-    run(out_first, 0, 1, 2, 3)
+    run(out_first, 0, 1)
+    conv_close()
     scope("qwait")
     weights_wait(2)
     scope("projectq")
@@ -699,6 +703,17 @@
                     at(sp=place, fs=2 * row + t, tp=core), jnp.logical_not(here),
                 )
 
+    run(out_first, 2, 3)
+    scope("statein")
+    arrived(st_in, s_recv)
+    scope("recnorm")
+    joined = inner + carried + lax.dot_general(
+        query_in, st_in[...], (((1,), (1,)), ((), ())), preferred_element_type=jnp.float32
+    )
+    joined = joined * lax.rsqrt(jnp.mean(joined * joined, axis=-1, keepdims=True) + EPS)
+    mix(0, joined * pk[2:3, :])
+
+    run(out_second, 0, 1)
     scope("statx")
     arrived(stat.at[pl.ds(0, 3)], c_recv)
     scope("cnorm")
@@ -710,16 +725,6 @@
     inv_c = dot_as(inv_r, eighth, 0, 0)
     out = (cacc[...] - mean_c) * inv_c * pk[3:4, :]
     mix(1, out * jax.nn.sigmoid(out))
-
-    run(out_second, 0, 1)
-    scope("statein")
-    arrived(st_in, s_recv)
-    scope("recnorm")
-    joined = inner + carried + lax.dot_general(
-        query_in, st_in[...], (((1,), (1,)), ((), ())), preferred_element_type=jnp.float32
-    )
-    joined = joined * lax.rsqrt(jnp.mean(joined * joined, axis=-1, keepdims=True) + EPS)
-    mix(0, joined * pk[2:3, :])
 
     run(out_second, 2, 3)
     run(out_third, 0, 1, 2, 3)

time: 46.6 us -> 46.3 us (level)
  no operation moved by 1% of the time
where the time goes in v3:
time: 46.3 us; the launch traced here: 46.1 us
  Pallas kernels  45.4 us (98%)
  local copies, waits for them, and re-layouts  0.71 us (2%)
    pallas_call x1, Pallas kernels, pair_body(): pl.pallas_call(pair_kernel, out_shape=pltpu.VMEM((1, rows, d), bf), in_sp...  45.4 us

profile of v3, /device:TPU:0, one launch (start us, length us, event | category | flops | bytes accessed | tf_op | source)
XLA Modules:
  0.0 46.1 jit_solution(16888787484299453536)
XLA Ops:
  0.0 45.4 %shard_map.145 = bf16[1,64,2048]{2,1,0:T(8,128)(2,1)S(1)} custom-call(bf16[1,64,2048]{2,1,0:T(8,128)(2,1)} %tokens_in.1, f32[1,2048]{1,0:T(1,128)} %bitcast.3, bf16[512,256]{1,0:T(8,128)(2,1)} %w0.1, bf16[512,256]{1,0:T(8,128)(2,1)} %w1.1, bf16[512,256]{1,0:T(8,128)(2,1)} %w2.1, bf16[512,256]{1,0:T(8,128)(2,1)} %w3.1, bf16[512,256]{1,0:T(8,128)(2,1)} %w4.1, ...), custom_call_target="tpu_custom_call" | custom-call | tf_op jit(solution)/shard_map/pallas_call | solution.py:830
  45.4 0.7 %copy.17 = bf16[1,64,2048]{2,1,0:T(8,128)(2,1)} copy(bf16[1,64,2048]{2,1,0:T(8,128)(2,1)S(1)} %shard_map.145) | data formatting | bytes 524288

commit v4 on v3

--- a/solution.py
+++ b/solution.py
@@ -735,18 +735,22 @@
     scope("ywait0")
     arrived(ya.at[:, pl.ds(0, groups)], a_recv.at[0])
     near_rows = aligned((1 - pair) * rows, rows, rows)
+    own_rows = aligned(pair * rows, rows, rows)
+
+    def product(at_rows, k):
+        at_n = pl.ds(k * cols, cols)
+        acc = jnp.dot(ya[at_rows, 0:groups], ow[0, :, at_n], preferred_element_type=jnp.float32)
+        acc = acc + jnp.dot(ya[at_rows, groups:], ow[1, :, at_n], preferred_element_type=jnp.float32)
+        return acc.astype(bf)
+
     for k in range(2):
-        scope(f"outmm{k}")
         if k == 1:
             arrived(ow.at[:, pl.ds(0, half), pl.ds(0, cols)], g_recv)
         at_n = pl.ds(k * cols, cols)
-        acc = jnp.dot(ya[:, 0:groups], ow[0, :, at_n], preferred_element_type=jnp.float32)
-        acc = acc + jnp.dot(ya[:, groups:], ow[1, :, at_n], preferred_element_type=jnp.float32)
-        mo[:, at_n] = acc.astype(bf)
+        mo[near_rows, at_n] = product(near_rows, k)
         send(mo.at[near_rows, at_n], fin.at[:, at_n], GIVE, f_recv.at[k], at(sp=near))
-    own_rows = aligned(pair * rows, rows, rows)
     for k, place in enumerate((s, far)):
-        o_ref[0, :, out_cols(place)] = mo[own_rows, pl.ds(k * cols, cols)]
+        o_ref[0, :, out_cols(place)] = product(own_rows, k)
     for k, place in enumerate((near, cross)):
         scope(f"give{k}")
         at_n = pl.ds(k * cols, cols)

time: 46.3 us -> 46.3 us (level)
  no operation moved by 1% of the time
where the time goes in v4:
time: 46.3 us; the launch traced here: 46.1 us
  Pallas kernels  45.4 us (98%)
  local copies, waits for them, and re-layouts  0.71 us (2%)
    pallas_call x1, Pallas kernels, pair_body(): pl.pallas_call(pair_kernel, out_shape=pltpu.VMEM((1, rows, d), bf), in_sp...  45.4 us

profile of v4, /device:TPU:0, one launch (start us, length us, event | category | flops | bytes accessed | tf_op | source)
XLA Modules:
  0.0 46.1 jit_solution(9850417479488001855)
XLA Ops:
  0.0 45.4 %shard_map.145 = bf16[1,64,2048]{2,1,0:T(8,128)(2,1)S(1)} custom-call(bf16[1,64,2048]{2,1,0:T(8,128)(2,1)} %tokens_in.1, f32[1,2048]{1,0:T(1,128)} %bitcast.3, bf16[512,256]{1,0:T(8,128)(2,1)} %w0.1, bf16[512,256]{1,0:T(8,128)(2,1)} %w1.1, bf16[512,256]{1,0:T(8,128)(2,1)} %w2.1, bf16[512,256]{1,0:T(8,128)(2,1)} %w3.1, bf16[512,256]{1,0:T(8,128)(2,1)} %w4.1, ...), custom_call_target="tpu_custom_call" | custom-call | tf_op jit(solution)/shard_map/pallas_call | solution.py:834
  45.4 0.7 %copy.17 = bf16[1,64,2048]{2,1,0:T(8,128)(2,1)} copy(bf16[1,64,2048]{2,1,0:T(8,128)(2,1)S(1)} %shard_map.145) | data formatting | bytes 524288
